TPU v7x, 32 devices: a whole 2x2x4 slice. The times are simulated.
32 devices in a mesh: sp: 8 (over z, y), tp: 4 (over x, core).
Axes of the slice: x: 2, y: 2, z: 4, core: 2. Of those that a mesh axis runs over, the one named last changes fastest.
Arguments:
- tokens: bfloat16 [4096, 2048], P('sp', 'tp'), may hold values from -6 to 6
- norm_gain: float32 [2048], replicated, may hold values from 0.1 to 1.9
- query_weight: bfloat16 [2048, 2048], P('sp', 'tp'), may hold values from -0.125 to 0.125
- key_weight: bfloat16 [2048, 512], P('sp', 'tp'), may hold values from -0.125 to 0.125
- value_weight: bfloat16 [2048, 512], P('sp', 'tp'), may hold values from -0.125 to 0.125
- pool_in_weight: bfloat16 [2048, 1024], P('sp', 'tp'), may hold values from -0.125 to 0.125
- pool_mix_weight: bfloat16 [4, 256, 256], P('tp'), may hold values from -0.375 to 0.375
- sink_logit: float32 [32], P('tp'), may hold values from -300 to 300
- out_pool_weight: bfloat16 [1024, 2048], P('tp', 'sp'), may hold values from -0.109375 to 0.109375
- out_attn_weight: bfloat16 [2048, 2048], P('tp', 'sp'), may hold values from -1.25 to 1.25
Outputs:
- mixed: bfloat16 [4096, 2048], P('sp', 'tp')
- log_weight: float32 [32, 4096], P('tp', 'sp')
All inputs are finite; a program needn't handle non-finite values.
Results may differ from a plain program's by a relative error of at most 0.012.
Values may be sent and summed in bfloat16 or wider, within the bound.
A program may use at most 64 MiB of HBM per device.

v0:
```python
import jax
import jax.numpy as jnp
from jax import lax
from jax.sharding import PartitionSpec as P

HD = 64
WINDOW = 128
GRID_W = 64


norm_eps = 1e-06
rope_base = 10000.0
pool_reach = 8
neg_fill = -1e30


def with_halo(cells, sides, width):
    for axis, dim in sides:
        count = lax.axis_size(axis)
        ends = count - 1
        head = lax.slice_in_dim(cells, 0, width, axis=dim)
        tail = lax.slice_in_dim(cells, cells.shape[dim] - width, cells.shape[dim], axis=dim)
        cells = jnp.concatenate(
            [
                lax.ppermute(tail, axis, [(i, (i + 1) % count) for i in range(ends)]),
                cells,
                lax.ppermute(head, axis, [((i + 1) % count, i) for i in range(ends)]),
            ],
            axis=dim,
        )
    return cells


def rope_tables(positions, head_dim):
    n_freq = head_dim // 4
    freqs = rope_base ** (-jnp.arange(n_freq, dtype=jnp.float32) / n_freq)
    rows = (positions // GRID_W).astype(jnp.float32)
    columns = (positions % GRID_W).astype(jnp.float32)
    row_angle = rows[:, None] * freqs[None, :]
    col_angle = columns[:, None] * freqs[None, :]
    return (jnp.cos(row_angle), jnp.sin(row_angle), jnp.cos(col_angle), jnp.sin(col_angle))


def rotate_half(values, cosine, sine):
    middle = values.shape[-1] // 2
    first = values[..., :middle]
    second = values[..., middle:]
    return jnp.concatenate([first * cosine - second * sine, second * cosine + first * sine], -1)


def rotate_heads(values, tables, head_dim):
    rows_count = values.shape[0]
    shaped = values.astype(jnp.float32).reshape(rows_count, -1, head_dim)
    cos_r, sin_r, cos_c, sin_c = [table[:, None, :] for table in tables]
    split = head_dim // 2
    turned = jnp.concatenate(
        [
            rotate_half(shaped[..., :split], cos_r, sin_r),
            rotate_half(shaped[..., split:], cos_c, sin_c),
        ],
        -1,
    )
    return turned.reshape(rows_count, -1).astype(jnp.bfloat16)


def pool_group(extended, own, positions, half_width, seq_total):
    rows_count = own.shape[0]
    summed = jnp.zeros(own.shape, jnp.float32)
    counted = jnp.zeros((rows_count,), jnp.float32)
    for shift_by in range(-pool_reach, pool_reach):
        source = positions + shift_by
        inside = (
            (shift_by >= -half_width)
            & (shift_by < half_width)
            & (source >= 0)
            & (source < seq_total)
        )
        window_rows = extended[pool_reach + shift_by : pool_reach + shift_by + rows_count].astype(
            jnp.float32
        )
        summed = summed + jnp.where(inside[:, None], window_rows, 0.0)
        counted = counted + inside.astype(jnp.float32)
    return (summed / counted[:, None] - own.astype(jnp.float32)).astype(jnp.bfloat16)


def attend_block(queries, keys, values, sink, query_pos, key_pos, seq_total):
    scores = jnp.einsum(
        "qhgd,khd->hgqk", queries, keys, preferred_element_type=jnp.float32
    ) * HD ** (-0.5)
    valid = (
        (jnp.abs(query_pos[:, None] - key_pos[None, :]) <= WINDOW)
        & (key_pos >= 0)[None, :]
        & (key_pos < seq_total)[None, :]
    )
    scores = jnp.where(valid, scores, neg_fill)
    row_top = jnp.maximum(jnp.max(scores, -1), sink[:, :, None])
    exps = jnp.exp(scores - row_top[..., None])
    row_total = jnp.sum(exps, -1) + jnp.exp(sink[:, :, None] - row_top)
    weights = (exps / row_total[..., None]).astype(jnp.bfloat16)
    attended = jnp.einsum("hgqk,khd->qhgd", weights, values, preferred_element_type=jnp.float32)
    return (attended.astype(jnp.bfloat16), row_top + jnp.log(row_total))


def fetch_outputs(out_pool_weight, out_attn_weight):
    return (
        lax.all_gather(out_pool_weight, "sp", axis=1, tiled=True),
        lax.all_gather(out_attn_weight, "sp", axis=1, tiled=True),
    )


def local(
    tokens,
    norm_gain,
    query_weight,
    key_weight,
    value_weight,
    pool_in_weight,
    pool_mix_weight,
    sink_logit,
    out_pool_weight,
    out_attn_weight,
):
    whole = lax.all_gather(tokens, "tp", axis=1, tiled=True)
    wide = whole.astype(jnp.float32)
    normed = (
        wide * lax.rsqrt(jnp.mean(wide * wide, -1, keepdims=True) + norm_eps) * norm_gain
    ).astype(jnp.bfloat16)
    tok_rows = normed.shape[0]
    seq_total = tok_rows * lax.axis_size("sp")
    offset = lax.axis_index("sp") * tok_rows
    weights_in = (query_weight, key_weight, value_weight, pool_in_weight)
    pieces = (
        lax.all_gather(weights_in[0], "sp", axis=0, tiled=True),
        lax.all_gather(weights_in[1], "sp", axis=0, tiled=True),
        lax.all_gather(weights_in[2], "sp", axis=0, tiled=True),
        lax.all_gather(weights_in[3], "sp", axis=0, tiled=True),
    )
    sums = tuple((jnp.dot(normed, piece, preferred_element_type=jnp.float32) for piece in pieces))
    query, key, value, pool_input = [total.astype(jnp.bfloat16) for total in sums]
    positions = offset + jnp.arange(tok_rows, dtype=jnp.int32)
    tables = rope_tables(positions, HD)
    rot_query = rotate_heads(query, tables, HD)
    rot_key = rotate_heads(key, tables, HD)
    key_width = rot_key.shape[1]
    pool_ext = with_halo(pool_input, (("sp", 0),), pool_reach)
    pair_ext = with_halo(jnp.concatenate([rot_key, value], 1), (("sp", 0),), WINDOW)
    key_ext = pair_ext[:, :key_width]
    value_ext = pair_ext[:, key_width:]
    half_width = jnp.left_shift(jnp.int32(1), lax.axis_index("tp"))
    pooled = pool_group(pool_ext, pool_input, positions, half_width, seq_total)
    pool_out = jnp.dot(pooled, pool_mix_weight[0], preferred_element_type=jnp.float32).astype(
        jnp.bfloat16
    )
    heads_local = rot_query.shape[1] // HD
    kv_local = key_width // HD
    grp = heads_local // kv_local
    query_heads = rot_query.reshape(tok_rows, kv_local, grp, HD)
    key_heads = key_ext.reshape(-1, kv_local, HD)
    value_heads = value_ext.reshape(-1, kv_local, HD)
    sink = sink_logit.reshape(kv_local, grp)
    block_rows = min(tok_rows, 256)
    attended_parts = []
    log_parts = []
    for block_index in range(tok_rows // block_rows):
        start = block_index * block_rows
        query_pos = offset + start + jnp.arange(block_rows, dtype=jnp.int32)
        key_pos = offset + start - WINDOW + jnp.arange(block_rows + 2 * WINDOW, dtype=jnp.int32)
        attended_block, log_block = attend_block(
            query_heads[start : start + block_rows],
            key_heads[start : start + block_rows + 2 * WINDOW],
            value_heads[start : start + block_rows + 2 * WINDOW],
            sink,
            query_pos,
            key_pos,
            seq_total,
        )
        attended_parts.append(attended_block.reshape(block_rows, heads_local * HD))
        log_parts.append(log_block.reshape(heads_local, block_rows))
    attended = jnp.concatenate(attended_parts, 0)
    log_weight = jnp.concatenate(log_parts, 1)
    out_pool_full, out_attn_full = fetch_outputs(out_pool_weight, out_attn_weight)
    term = jnp.dot(pool_out, out_pool_full, preferred_element_type=jnp.float32)
    term = term + jnp.dot(attended, out_attn_full, preferred_element_type=jnp.float32)
    mixed = lax.psum_scatter(term.astype(jnp.bfloat16), "tp", scatter_dimension=1, tiled=True)
    return (mixed, log_weight)


def solution(mesh):
    return jax.shard_map(
        local,
        mesh=mesh,
        in_specs=(
            P("sp", "tp"),
            P(),
            P("sp", "tp"),
            P("sp", "tp"),
            P("sp", "tp"),
            P("sp", "tp"),
            P("tp", None, None),
            P("tp"),
            P("tp", "sp"),
            P("tp", "sp"),
        ),
        out_specs=(P("sp", "tp"), P("tp", "sp")),
        check_vma=False,
    )
```

profile of v0, /device:TPU:19, one launch (start us, length us, event | category | flops | bytes accessed | tf_op | source)
XLA Modules:
  0.0 260.2 jit_solution(8358394788098384605)
XLA Ops:
  7.2 0.0 all-gather.6.cloned.1.call-start
  7.2 0.7 all-gather.6.cloned.1.call-update
  7.9 0.0 all-gather.8.cloned.1.call-start
  8.0 0.7 all-gather.8.cloned.1.call-update
  8.7 0.0 all-gather.10.cloned.1.call-start
  8.7 0.7 all-gather.10.cloned.1.call-update
  9.4 0.0 all-gather.12.cloned.1.call-start
  9.4 0.5 all-gather.12.cloned.1.call-update
  10.0 0.0 all-gather.14.cloned.1.call-start
  10.0 0.5 all-gather.14.cloned.1.call-update
  10.6 0.0 reduce-scatter.2.cloned.1.call-start
  10.8 22.1 %all_gather.24 = bf16[2048,128]{1,0:T(8,128)(2,1)S(1)} all-gather(bf16[256,128]{1,0:T(8,128)(2,1)} %param.13), channel_id=1, replica_groups=mesh['sp'=8,'tp'=4] {'sp'}, dimensions={0}, use_global_device_ids=true | all-gather | bytes 589824 | tf_op jit(solution)/shard_map/all_gather | solution.py:134
  32.9 26.4 %all_gather.25 = bf16[2048,128]{1,0:T(8,128)(2,1)S(1)} all-gather(bf16[256,128]{1,0:T(8,128)(2,1)} %param.14), channel_id=1, replica_groups=mesh['sp'=8,'tp'=4] {'sp'}, dimensions={0}, use_global_device_ids=true | all-gather | bytes 589824 | tf_op jit(solution)/shard_map/all_gather | solution.py:135
  59.3 0.7 max.38
  60.0 0.9 multiply_cosine_fusion.1
  61.0 0.3 fusion.25
  61.2 0.3 fusion.27
  61.5 0.7 convert_add_fusion
  62.2 2.2 fusion
  64.5 2.5 convolution_convert_fusion.4
  67.1 7.8 %all-gather.8.cloned.1.call-done = bf16[2048,256]{1,0:T(8,128)(2,1)} async-done(((bf16[256,256]{1,0:T(8,128)(2,1)}), bf16[2048,256]{1,0:T(8,128)(2,1)}) %all-gather.8.cloned.1.call-update) | async-done | bytes 1048592 | tf_op jit(solution)/shard_map/all_gather | solution.py:136
  74.8 2.0 convolution_convert_fusion.2
  76.9 2.9 %collective-permute-start = (bf16[8,256]{1,0:T(8,128)(2,1)S(1)}, bf16[8,256]{1,0:T(8,128)(2,1)}, u32[]{:S(2)}, u32[]{:S(2)}) collective-permute-start(bf16[8,256]{1,0:T(8,128)(2,1)S(1)} %get-tuple-element.41), channel_id=1, source_target_pairs={{0,4},{4,8},{8,12},{12,16},{16,20},{20,24},{24,28},{1,5},{5,9},{9,... | collective-permute-start | bytes 12296 | tf_op jit(solution)/shard_map/ppermute | solution.py:25
  79.7 3.3 %collective-permute-start.1 = (bf16[8,256]{1,0:T(8,128)(2,1)S(1)}, bf16[8,256]{1,0:T(8,128)(2,1)}, u32[]{:S(2)}, u32[]{:S(2)}) collective-permute-start(bf16[8,256]{1,0:T(8,128)(2,1)S(1)} %get-tuple-element.42), channel_id=1, source_target_pairs={{4,0},{8,4},{12,8},{16,12},{20,16},{24,20},{28,24},{5,1},{9,5},{13... | collective-permute-start | bytes 12296 | tf_op jit(solution)/shard_map/ppermute | solution.py:27
  83.2 1.6 convolution_convert_fusion.3
  84.8 2.0 collective-permute-start.2
  86.8 4.4 %collective-permute-start.3 = (bf16[128,256]{0,1:T(8,128)(2,1)S(1)}, bf16[128,256]{0,1:T(8,128)(2,1)S(1)}, u32[]{:S(2)}, u32[]{:S(2)}) collective-permute-start(bf16[128,256]{0,1:T(8,128)(2,1)S(1)} %get-tuple-element.38), channel_id=1, source_target_pairs={{4,0},{8,4},{12,8},{16,12},{20,16},{24,20},{28,24},{5,1},{9,5},{13... | collective-permute-start | bytes 196616 | tf_op jit(solution)/shard_map/ppermute | solution.py:27
  91.2 25.4 %all-gather.10.cloned.1.call-done = bf16[256,2048]{1,0:T(8,128)(2,1)} async-done(((bf16[256,256]{1,0:T(8,128)(2,1)}), bf16[256,2048]{1,0:T(8,128)(2,1)}) %all-gather.10.cloned.1.call-update) | async-done | bytes 1048592 | tf_op jit(solution)/shard_map/all_gather | solution.py:106
  116.6 8.6 %fusion.11 = f32[512,2048]{1,0:T(8,128)} fusion(bf16[256,2048]{1,0:T(8,128)(2,1)} %all-gather.10.cloned.1.call-done, bf16[512,256]{1,0:T(8,128)(2,1)} %copy-done.9, bf16[8,256]{1,0:T(8,128)(2,1)} %collective-permute-done.1, bf16[8,256]{1,0:T(8,128)(2,1)} %collective-permute-done, f32[512]{0:T(512)S(1)} %get-tuple-element.2, ...), kind=kOutput, calls=%fused_computation.23 | convolution fusion | flops 616562688 | bytes 5654528 | tf_op jit(solution)/shard_map/dot_general | solution.py:182
  125.3 42.1 %all-gather.12.cloned.1.call-done = bf16[2048,512]{1,0:T(8,128)(2,1)} async-done(((bf16[256,512]{1,0:T(8,128)(2,1)}), bf16[2048,512]{1,0:T(8,128)(2,1)}) %all-gather.12.cloned.1.call-update) | async-done | bytes 2097168 | tf_op jit(solution)/shard_map/all_gather | solution.py:133
  167.4 3.0 %convolution_convert_fusion = bf16[512,512]{0,1:T(8,128)(2,1)S(1)} fusion(bf16[2048,512]{1,0:T(8,128)(2,1)} %all-gather.12.cloned.1.call-done, bf16[512,2048]{1,0:T(8,128)(2,1)S(1)} %copy-done.1, f32[2048]{0:T(1024)} %param.11, f32[512]{0:T(512)S(1)} %copy-done.7), kind=kOutput, calls=%fused_computation.18 | convolution fusion | flops 1078198272 | bytes 4728832 | tf_op jit(solution)/shard_map/dot_general | solution.py:138
  170.4 0.1 convert.35
  170.5 0.2 subtract_convert_fusion.1
  170.8 0.8 fusion.5
  171.6 0.1 broadcast_maximum_fusion.1
  171.7 0.8 fusion.6
  172.5 0.9 fusion.3
  173.4 0.1 exponential_add_fusion.1
  173.5 0.9 fusion.4
  174.3 0.1 exponential_add_fusion
  174.4 1.2 fusion.10
  175.7 1.2 fusion.9
  176.9 40.9 %all-gather.14.cloned.1.call-done = bf16[512,2048]{1,0:T(8,128)(2,1)} async-done(((bf16[512,256]{1,0:T(8,128)(2,1)}), bf16[512,2048]{1,0:T(8,128)(2,1)}) %all-gather.14.cloned.1.call-update) | async-done | bytes 2097168 | tf_op jit(solution)/shard_map/all_gather | solution.py:107
  217.8 5.5 %add_convert_fusion = bf16[512,2048]{1,0:T(8,128)(2,1)} fusion(f32[512,2048]{1,0:T(8,128)} %fusion.11, bf16[512,2048]{1,0:T(8,128)(2,1)} %all-gather.14.cloned.1.call-done, bf16[256,512]{0,1:T(8,128)(2,1)S(1)} %bitcast.79, bf16[256,512]{0,1:T(8,128)(2,1)S(1)} %bitcast.78), kind=kOutput, calls=%fused_computation.7 | convolution fusion | flops 1076887552 | bytes 8912896 | tf_op jit(solution)/shard_map/dot_general | solution.py:183
  223.3 0.0 reduce-scatter.2.cloned.1.call-update
  223.4 0.1 log_add_fusion.1
  223.5 0.6 pad_maximum_fusion.16
  224.1 29.3 %reduce-scatter.2.cloned.1.call-done = bf16[512,512]{1,0:T(8,128)(2,1)} async-done(((bf16[512,2048]{1,0:T(8,128)(2,1)}), bf16[512,512]{1,0:T(8,128)(2,1)}) %reduce-scatter.2.cloned.1.call-update) | async-done | bytes 524304 | tf_op jit(solution)/shard_map/reduce_scatter | solution.py:184
  (48 shorter events, 0.4 us)
Async XLA Ops:
  7.2 109.4 %copy-start = (bf16[1,256,256]{2,1,0:T(8,128)(2,1)S(1)}, bf16[1,256,256]{2,1,0:T(8,128)(2,1)}, u32[]{:S(2)}) copy-start(bf16[1,256,256]{2,1,0:T(8,128)(2,1)} %param.16) | copy-start | bytes 393220
  7.2 55.0 %all-gather.6.cloned.1.call-start = ((), (), s32[]{:S(2)}) async-start(), calls=%async_computation.1 | async-start | bytes 2621440 | tf_op jit(solution)/shard_map/all_gather | solution.py:123
  7.9 66.9 %all-gather.8.cloned.1.call-start = ((), (), s32[]{:S(2)}) async-start(), calls=%async_computation.2 | async-start | bytes 1179648 | tf_op jit(solution)/shard_map/all_gather | solution.py:136
  8.7 107.9 %all-gather.10.cloned.1.call-start = ((), (), s32[]{:S(2)}) async-start(), calls=%async_computation.3 | async-start | bytes 1179648 | tf_op jit(solution)/shard_map/all_gather | solution.py:106
  9.4 158.0 %all-gather.12.cloned.1.call-start = ((), (), s32[]{:S(2)}) async-start(), calls=%async_computation.4 | async-start | bytes 2359296 | tf_op jit(solution)/shard_map/all_gather | solution.py:133
  10.0 207.8 %all-gather.14.cloned.1.call-start = ((), (), s32[]{:S(2)}) async-start(), calls=%async_computation.5 | async-start | bytes 2359296 | tf_op jit(solution)/shard_map/all_gather | solution.py:107
  10.6 242.8 %reduce-scatter.2.cloned.1.call-start = ((), (), s32[]{:S(2)}) async-start(), calls=%async_computation.6 | async-start | bytes 2621440 | tf_op jit(solution)/shard_map/reduce_scatter | solution.py:184
  62.2 12.6 %copy-start.1 = (bf16[512,2048]{1,0:T(8,128)(2,1)S(1)}, bf16[512,2048]{1,0:T(8,128)(2,1)}, u32[]{:S(2)}) copy-start(bf16[512,2048]{1,0:T(8,128)(2,1)} %all-gather.6.cloned.1.call-done) | copy-start | bytes 6291460
  64.5 10.4 %copy-start.6 = (f32[512]{0:T(512)}, f32[512]{0:T(512)S(1)}, u32[]{:S(2)}) copy-start(f32[512]{0:T(512)S(1)} %add_rsqrt_fusion) | copy-start | bytes 6148
  67.0 16.1 %copy-start.2 = (f32[512,16]{0,1:T(8,128)S(1)}, f32[512,16]{0,1:T(8,128)}, u32[]{:S(2)}) copy-start(f32[512,16]{0,1:T(8,128)} %get-tuple-element.43) | copy-start | bytes 98308
  67.0 16.1 %copy-start.3 = (f32[512,16]{0,1:T(8,128)S(1)}, f32[512,16]{0,1:T(8,128)}, u32[]{:S(2)}) copy-start(f32[512,16]{0,1:T(8,128)} %get-tuple-element.44) | copy-start | bytes 98308
  67.0 16.1 %copy-start.4 = (f32[512,16]{0,1:T(8,128)S(1)}, f32[512,16]{0,1:T(8,128)}, u32[]{:S(2)}) copy-start(f32[512,16]{0,1:T(8,128)} %get-tuple-element.51) | copy-start | bytes 98308
  67.0 16.1 %copy-start.5 = (f32[512,16]{0,1:T(8,128)S(1)}, f32[512,16]{0,1:T(8,128)}, u32[]{:S(2)}) copy-start(f32[512,16]{0,1:T(8,128)} %get-tuple-element.52) | copy-start | bytes 98308
  67.0 16.1 %copy-start.10 = (f32[2048]{0:T(1024)S(1)}, f32[2048]{0:T(1024)}, u32[]{:S(2)}) copy-start(f32[2048]{0:T(1024)} %param.11) | copy-start | bytes 24580
  76.8 6.3 %copy-start.9 = (bf16[512,256]{1,0:T(8,128)(2,1)}, bf16[512,256]{1,0:T(8,128)(2,1)S(1)}, u32[]{:S(2)}) copy-start(bf16[512,256]{1,0:T(8,128)(2,1)S(1)} %convolution_convert_fusion.2) | copy-start | bytes 786436
  76.9 39.7 %collective-permute-start = (bf16[8,256]{1,0:T(8,128)(2,1)S(1)}, bf16[8,256]{1,0:T(8,128)(2,1)}, u32[]{:S(2)}, u32[]{:S(2)}) collective-permute-start(bf16[8,256]{1,0:T(8,128)(2,1)S(1)} %get-tuple-element.41), channel_id=1, source_target_pairs={{0,4},{4,8},{8,12},{12,16},{16,20},{20,24},{24,28},{1,5},{5,9},{9,... | collective-permute-start | bytes 12296 | tf_op jit(solution)/shard_map/ppermute | solution.py:25
  79.7 36.8 %collective-permute-start.1 = (bf16[8,256]{1,0:T(8,128)(2,1)S(1)}, bf16[8,256]{1,0:T(8,128)(2,1)}, u32[]{:S(2)}, u32[]{:S(2)}) collective-permute-start(bf16[8,256]{1,0:T(8,128)(2,1)S(1)} %get-tuple-element.42), channel_id=1, source_target_pairs={{4,0},{8,4},{12,8},{16,12},{20,16},{24,20},{28,24},{5,1},{9,5},{13... | collective-permute-start | bytes 12296 | tf_op jit(solution)/shard_map/ppermute | solution.py:27
  84.8 40.4 %collective-permute-start.2 = (bf16[128,256]{0,1:T(8,128)(2,1)S(1)}, bf16[128,256]{0,1:T(8,128)(2,1)S(1)}, u32[]{:S(2)}, u32[]{:S(2)}) collective-permute-start(bf16[128,256]{0,1:T(8,128)(2,1)S(1)} %get-tuple-element.37), channel_id=1, source_target_pairs={{0,4},{4,8},{8,12},{12,16},{16,20},{20,24},{24,28},{1,5},{5,9},{9,... | collective-permute-start | bytes 196616 | tf_op jit(solution)/shard_map/ppermute | solution.py:25
  86.8 38.5 %collective-permute-start.3 = (bf16[128,256]{0,1:T(8,128)(2,1)S(1)}, bf16[128,256]{0,1:T(8,128)(2,1)S(1)}, u32[]{:S(2)}, u32[]{:S(2)}) collective-permute-start(bf16[128,256]{0,1:T(8,128)(2,1)S(1)} %get-tuple-element.38), channel_id=1, source_target_pairs={{4,0},{8,4},{12,8},{16,12},{20,16},{24,20},{28,24},{5,1},{9,5},{13... | collective-permute-start | bytes 196616 | tf_op jit(solution)/shard_map/ppermute | solution.py:27
  116.6 50.8 %copy-start.7 = (f32[512]{0:T(512)S(1)}, f32[512]{0:T(512)}, u32[]{:S(2)}) copy-start(f32[512]{0:T(512)} %copy-done.6) | copy-start | bytes 6148
  217.8 5.6 %copy-start.8 = (f32[8]{0:T(128)S(1)}, f32[8]{0:T(128)}, u32[]{:S(2)}) copy-start(f32[8]{0:T(128)} %param.17) | copy-start | bytes 100
Sparse Core Ops, SparseCore 0:
  9.5 23.0 all-gather.5
  34.8 39.9 all-gather.7
  76.9 39.6 all-gather.9
  118.5 48.7 all-gather.11
  169.3 48.4 all-gather.13
  223.4 29.8 reduce-scatter.1
where the time goes:
time: 263 us; the launch traced here: 260 us
  waiting for transfers between devices  149 us (57%)
  blocking collectives  48.5 us (18%)
  matrix products  27.3 us (10%)
  between operations  14.6 us (6%)
  starting transfers between devices  12.8 us (5%)
  other arithmetic  7.62 us (3%)
    all_gather x1, waiting for transfers between devices, local(): lax.all_gather(weights_in[0], 'sp', axis=0, tiled=True)  42.1 us
    all_gather x1, waiting for transfers between devices, fetch_outputs(): lax.all_gather(out_attn_weight, 'sp', axis=1, tiled=True)  40.9 us
    reduce_scatter x1, waiting for transfers between devices, local(): lax.psum_scatter(term.astype(jnp.bfloat16), 'tp', scatter_dimension=1, ti...  29.3 us
    all_gather x1, blocking collectives, local(): lax.all_gather(weights_in[2], 'sp', axis=0, tiled=True)  26.4 us
    all_gather x1, waiting for transfers between devices, fetch_outputs(): lax.all_gather(out_pool_weight, 'sp', axis=1, tiled=True)  25.4 us
    all_gather x1, blocking collectives, local(): lax.all_gather(weights_in[1], 'sp', axis=0, tiled=True)  22.1 us
    dot_general x4, matrix products, local(): jnp.dot(normed, piece, preferred_element_type=jnp.float32)  9.07 us
    dot_general x1, matrix products, local(): term = jnp.dot(pool_out, out_pool_full, preferred_element_type=jnp.float32)  8.65 us
  transfers between devices with their start and end apart: 10, of which 5 were waited for; matrix products, arithmetic and copies ran while one was open for 12% of the time, Pallas kernels for 0%

commit v1 on v0

--- a/solution.py
+++ b/solution.py
@@ -1,6 +1,10 @@
+import functools
+
 import jax
 import jax.numpy as jnp
 from jax import lax
+from jax.experimental import pallas as pl
+from jax.experimental.pallas import tpu as pltpu
 from jax.sharding import PartitionSpec as P
 
 HD = 64
@@ -185,9 +189,493 @@
     return (mixed, log_weight)
 
 
+NY = 2
+PIECES = 2
+MESH = pl.DeviceIdType.MESH
+
+
+def layer_kernel(
+    nz,
+    ntp,
+    tok_ref,
+    gain_ref,
+    qw_ref,
+    kw_ref,
+    vw_ref,
+    pw_ref,
+    mix_ref,
+    sink_ref,
+    ow_ref,
+    aw_ref,
+    cos_ref,
+    sin_ref,
+    mixed_ref,
+    log_ref,
+    xg,
+    normed,
+    wg,
+    wo,
+    qrot,
+    ext,
+    act,
+    part,
+    rsb,
+    loc_sem,
+    w_send,
+    w_recv,
+    x_send,
+    x_recv,
+    h_send,
+    h_recv,
+    r_send,
+    r_recv,
+):
+    sp, tp = lax.axis_index("sp"), lax.axis_index("tp")
+    nsp = nz * NY
+    z, y = sp // NY, sp % NY
+    rows = tok_ref.shape[0]
+    width = tok_ref.shape[1]
+    brow = qw_ref.shape[0]
+    qn, kn, pn = qw_ref.shape[1], kw_ref.shape[1], pw_ref.shape[1]
+    pool_rows = ow_ref.shape[0]
+    fan = wo.shape[1]
+    ocols = wo.shape[2]
+    seq_total = rows * nsp
+    heads, kv_local = qn // HD, kn // HD
+    grp = heads // kv_local
+
+    base = pl.multiple_of(sp * brow, brow)
+    own = [
+        (tok_ref, xg.at[tp]),
+        (qw_ref, wg.at[pl.ds(base, brow), pl.ds(0, qn)]),
+        (kw_ref, wg.at[pl.ds(base, brow), pl.ds(qn, kn)]),
+        (vw_ref, wg.at[pl.ds(base, brow), pl.ds(qn + kn, kn)]),
+        (pw_ref, wg.at[pl.ds(base, brow), pl.ds(qn + 2 * kn, pn)]),
+        (ow_ref, wo.at[sp, pl.ds(0, pool_rows)]),
+        (aw_ref, wo.at[sp, pl.ds(pool_rows, fan - pool_rows)]),
+    ]
+    local_copies = [pltpu.make_async_copy(a, b, loc_sem.at[i]) for i, (a, b) in enumerate(own)]
+    for copy in local_copies:
+        copy.start()
+    ext[...] = jnp.zeros_like(ext)
+
+    barrier = pltpu.get_barrier_semaphore()
+    sp_peers = [
+        (z + 1 < nz, sp + NY),
+        (z >= 1, sp - NY),
+        (z >= 0, z * NY + (1 - y)),
+        (sp + 1 < nsp, sp + 1),
+        (sp >= 1, sp - 1),
+    ]
+    expected = ntp - 1
+    for ok, peer in sp_peers:
+        expected = expected + ok.astype(jnp.int32)
+
+        @pl.when(ok)
+        def _():
+            pl.semaphore_signal(barrier, inc=1, device_id={"sp": peer}, device_id_type=MESH)
+
+    for step in range(1, ntp):
+        other = lax.rem(tp + step, ntp)
+        pl.semaphore_signal(barrier, inc=1, device_id={"tp": other}, device_id_type=MESH)
+    for copy in local_copies:
+        copy.wait()
+    pl.semaphore_wait(barrier, expected)
+
+    def weight_copy(kind, block, piece, way):
+        if kind == 0:
+            size = brow // PIECES
+            start = pl.multiple_of(block * brow + piece * size, size)
+            ref = wg.at[pl.ds(start, size)]
+        else:
+            size = fan // PIECES
+            ref = wo.at[block, pl.ds(piece * size, size)]
+        target = (sp + NY, sp - NY, z * NY + (1 - y))[way]
+        return pltpu.make_async_remote_copy(
+            src_ref=ref,
+            dst_ref=ref,
+            send_sem=w_send.at[kind, way, block, piece],
+            recv_sem=w_recv.at[kind, block, piece],
+            device_id={"sp": target},
+            device_id_type=MESH,
+        )
+
+    onward = (z + 1 < nz, z >= 1)
+
+    def relay(kind, d, done=False):
+        def act_on(copy):
+            if done:
+                copy.wait_send()
+            else:
+                copy.start()
+
+        for piece in range(PIECES):
+            for way in range(2):
+                source = (z - d, z + d)[way]
+                block = source * NY + y
+                if d == 0:
+                    @pl.when(onward[way])
+                    def _():
+                        act_on(weight_copy(kind, block, piece, way))
+
+                    if way == 1:
+                        act_on(weight_copy(kind, block, piece, 2))
+                else:
+                    valid = (source >= 0) & (source < nz)
+
+                    @pl.when(valid)
+                    def _():
+                        if not done:
+                            weight_copy(kind, block, piece, 2).wait_recv()
+
+                        @pl.when(onward[way])
+                        def _():
+                            act_on(weight_copy(kind, block, piece, way))
+
+                        act_on(weight_copy(kind, block, piece, 2))
+
+    def token_copy(step):
+        other = lax.rem(tp + step, ntp)
+        return pltpu.make_async_remote_copy(
+            src_ref=xg.at[tp],
+            dst_ref=xg.at[tp],
+            send_sem=x_send.at[step],
+            recv_sem=x_recv.at[tp],
+            device_id={"tp": other},
+            device_id_type=MESH,
+        )
+
+    def token_wait(step):
+        other = lax.rem(tp + step, ntp)
+        return pltpu.make_async_remote_copy(
+            src_ref=xg.at[other],
+            dst_ref=xg.at[other],
+            send_sem=x_send.at[step],
+            recv_sem=x_recv.at[other],
+            device_id={"tp": other},
+            device_id_type=MESH,
+        )
+
+    relay(0, 0)
+    for step in range(1, ntp):
+        token_copy(step).start()
+    for d in range(1, nz - 1):
+        relay(0, d)
+
+    for step in range(1, ntp):
+        token_wait(step).wait_recv()
+
+    norm_rows = 64
+
+    @pl.loop(0, rows // norm_rows)
+    def _(i):
+        at = pl.ds(pl.multiple_of(i * norm_rows, norm_rows), norm_rows)
+        pieces = [xg[t, at, :].astype(jnp.float32) for t in range(ntp)]
+        total = sum(jnp.sum(piece * piece, -1, keepdims=True) for piece in pieces)
+        scale = lax.rsqrt(total / (width * ntp) + norm_eps)
+        for t in range(ntp):
+            cols = pl.ds(t * width, width)
+            normed[at, cols] = (pieces[t] * scale * gain_ref[:, cols]).astype(jnp.bfloat16)
+
+    for d in range(max(nz - 1, 1), nz):
+        relay(0, d)
+    relay(1, 0)
+    for d in range(1, min(nz, 2)):
+        relay(1, d)
+
+    for source in range(nz):
+        for piece in range(PIECES):
+            weight_copy(0, source * NY + (1 - y), piece, 2).wait_recv()
+
+    half = HD // 4
+    lane = lax.broadcasted_iota(jnp.int32, (rows, 128), 1)
+    is_first = (lane % (2 * half)) < half
+
+    def turn(values, factor):
+        wide = values.astype(jnp.bfloat16).astype(jnp.float32)
+        swapped = jnp.where(
+            is_first, pltpu.roll(wide, 128 - half, 1), pltpu.roll(wide, half, 1)
+        )
+        return ((wide * cos_ref[...] + swapped * sin_ref[...]) * factor).astype(jnp.bfloat16)
+
+    def project(start, size):
+        return jnp.dot(normed[...], wg[:, start : start + size], preferred_element_type=jnp.float32)
+
+    mid = pl.ds(WINDOW, rows)
+    for c in range(0, kn, 128):
+        ext[mid, c : c + 128] = turn(project(qn + c, 128), 1.0)
+    ext[mid, kn : 2 * kn] = project(qn + kn, kn).astype(jnp.bfloat16)
+    ext[mid, 2 * kn : 2 * kn + pn] = project(qn + 2 * kn, pn).astype(jnp.bfloat16)
+    for c in range(0, qn, 256):
+        both = project(qn * 0 + c, 256)
+        qrot[:, c : c + 128] = turn(both[:, :128], HD ** -0.5)
+        qrot[:, c + 128 : c + 256] = turn(both[:, 128:], HD ** -0.5)
+
+    edge = 16
+
+    def halo_copy(way, what):
+        cols = pl.ds(0, 2 * kn) if what == 0 else pl.ds(2 * kn, pn)
+        count = WINDOW if what == 0 else edge
+        if way == 0:
+            src, dst = WINDOW + rows - count, WINDOW - count
+            target = sp + 1
+        else:
+            src, dst = WINDOW, WINDOW + rows
+            target = sp - 1
+        return pltpu.make_async_remote_copy(
+            src_ref=ext.at[pl.ds(src, count), cols],
+            dst_ref=ext.at[pl.ds(dst, count), cols],
+            send_sem=h_send.at[way, what],
+            recv_sem=h_recv.at[way, what],
+            device_id={"sp": target},
+            device_id_type=MESH,
+        )
+
+    has_next, has_prev = sp + 1 < nsp, sp >= 1
+
+    for way, ok in ((0, has_next), (1, has_prev)):
+        @pl.when(ok)
+        def _():
+            halo_copy(way, 0).start()
+            halo_copy(way, 1).start()
+
+    span = 3 * WINDOW
+    row_at = lax.broadcasted_iota(jnp.int32, (WINDOW, span), 0)
+    key_at = lax.broadcasted_iota(jnp.int32, (WINDOW, span), 1)
+    half_width = jnp.left_shift(jnp.int32(1), tp)
+
+    def mixer_block(i):
+        q_at = slice(i * WINDOW, (i + 1) * WINDOW)
+        window = slice(i * WINDOW, i * WINDOW + span)
+        first = sp * rows + (i - 1) * WINDOW
+        inside = (key_at + first >= 0) & (key_at + first < seq_total)
+        apart = key_at - row_at
+        band = inside & (apart >= WINDOW - half_width) & (apart < WINDOW + half_width)
+        band_f = band.astype(jnp.float32)
+        counted = jnp.sum(band_f, -1, keepdims=True)
+        summed = jnp.dot(
+            band_f.astype(jnp.bfloat16),
+            ext[window, 2 * kn : 2 * kn + pn],
+            preferred_element_type=jnp.float32,
+        )
+        own_pool = ext[(i + 1) * WINDOW : (i + 2) * WINDOW, 2 * kn : 2 * kn + pn]
+        pooled = (summed / counted - own_pool.astype(jnp.float32)).astype(jnp.bfloat16)
+        act[q_at, 0:pn] = jnp.dot(
+            pooled, mix_ref[...], preferred_element_type=jnp.float32
+        ).astype(jnp.bfloat16)
+        valid = inside & (apart >= 0) & (apart <= 2 * WINDOW)
+        logs = jnp.zeros((WINDOW, 128), jnp.float32)
+        lane_at = lax.broadcasted_iota(jnp.int32, (WINDOW, 128), 1)
+        for kv in range(kv_local):
+            keys = ext[window, kv * HD : (kv + 1) * HD]
+            values = ext[window, kn + kv * HD : kn + (kv + 1) * HD]
+            outs = []
+            for g in range(grp):
+                head = kv * grp + g
+                query = qrot[q_at, head * HD : (head + 1) * HD]
+                score = lax.dot_general(
+                    query, keys, (((1,), (1,)), ((), ())), preferred_element_type=jnp.float32
+                )
+                score = jnp.where(valid, score, neg_fill)
+                sink = sink_ref[head]
+                top = jnp.maximum(jnp.max(score, -1, keepdims=True), sink)
+                exps = jnp.exp(score - top)
+                total = jnp.sum(exps, -1, keepdims=True) + jnp.exp(sink - top)
+                weights = (exps * (1.0 / total)).astype(jnp.bfloat16)
+                outs.append(jnp.dot(weights, values, preferred_element_type=jnp.float32))
+                logs = jnp.where(lane_at == head, top + jnp.log(total), logs)
+            for g in range(0, grp, 2):
+                at = pn + (kv * grp + g) * HD
+                act[q_at, at : at + 2 * HD] = jnp.concatenate(outs[g : g + 2], 1).astype(
+                    jnp.bfloat16
+                )
+        log_ref[:, q_at] = logs.T[:heads, :]
+
+    n_blocks = rows // WINDOW
+    for i in range(1, n_blocks - 1):
+        mixer_block(i)
+        if i == 1:
+            for d in range(2, min(nz, 3)):
+                relay(1, d)
+    for way, ok in ((0, has_prev), (1, has_next)):
+        @pl.when(ok)
+        def _():
+            halo_copy(way, 0).wait_recv()
+            halo_copy(way, 1).wait_recv()
+
+    for i in (0, n_blocks - 1):
+        mixer_block(i)
+        if i == 0:
+            for d in range(3, nz):
+                relay(1, d)
+
+    per_owner = nsp // ntp
+
+    def reduce_copy(block):
+        owner = block // per_owner
+        slot = block % per_owner
+        return pltpu.make_async_remote_copy(
+            src_ref=part.at[block],
+            dst_ref=rsb.at[tp, slot],
+            send_sem=r_send.at[block],
+            recv_sem=r_recv.at[tp, slot],
+            device_id={"tp": owner},
+            device_id_type=MESH,
+        )
+
+    def out_block(block):
+        part[block] = jnp.dot(act[...], wo[block], preferred_element_type=jnp.float32).astype(
+            jnp.bfloat16
+        )
+
+        @pl.when(block // per_owner != tp)
+        def _():
+            reduce_copy(block).start()
+
+    @pl.loop(0, nz)
+    def _(j):
+        out_block(j * NY + y)
+
+    @pl.loop(0, 2 * nz - 1)
+    def _(k):
+        d = (k + 1) // 2
+        source = z + (1 - 2 * (k % 2)) * d
+
+        @pl.when((source >= 0) & (source < nz))
+        def _():
+            block = source * NY + (1 - y)
+            for piece in range(PIECES):
+                weight_copy(1, block, piece, 2).wait_recv()
+            out_block(block)
+
+    for step in range(1, ntp):
+        other = lax.rem(tp + step, ntp)
+        for slot in range(per_owner):
+            pltpu.make_async_remote_copy(
+                src_ref=rsb.at[other, slot],
+                dst_ref=rsb.at[other, slot],
+                send_sem=r_send.at[slot],
+                recv_sem=r_recv.at[other, slot],
+                device_id={"tp": other},
+                device_id_type=MESH,
+            ).wait_recv()
+    for slot in range(per_owner):
+        total = part[tp * per_owner + slot].astype(jnp.float32)
+        for step in range(1, ntp):
+            total = total + rsb[lax.rem(tp + step, ntp), slot].astype(jnp.float32)
+        mixed_ref[:, slot * ocols : (slot + 1) * ocols] = total.astype(jnp.bfloat16)
+
+    for step in range(1, ntp):
+        token_copy(step).wait_send()
+    for kind in range(2):
+        for d in range(nz):
+            relay(kind, d, done=True)
+    for way, ok in ((0, has_next), (1, has_prev)):
+        @pl.when(ok)
+        def _():
+            halo_copy(way, 0).wait_send()
+            halo_copy(way, 1).wait_send()
+
+    @pl.loop(0, nsp)
+    def _(block):
+        @pl.when(block // per_owner != tp)
+        def _():
+            reduce_copy(block).wait_send()
+
+
+def fused(
+    nz,
+    ntp,
+    tokens,
+    norm_gain,
+    query_weight,
+    key_weight,
+    value_weight,
+    pool_in_weight,
+    pool_mix_weight,
+    sink_logit,
+    out_pool_weight,
+    out_attn_weight,
+):
+    rows, width = tokens.shape
+    nsp = nz * NY
+    dim = width * ntp
+    qn, kn, pn = query_weight.shape[1], key_weight.shape[1], pool_in_weight.shape[1]
+    fan = out_pool_weight.shape[0] + out_attn_weight.shape[0]
+    ocols = out_pool_weight.shape[1]
+    positions = lax.axis_index("sp") * rows + jnp.arange(rows, dtype=jnp.int32)
+    cos_r, sin_r, cos_c, sin_c = rope_tables(positions, HD)
+    cosine = jnp.tile(jnp.concatenate([cos_r, cos_r, cos_c, cos_c], 1), (1, 128 // HD))
+    sine = jnp.tile(jnp.concatenate([-sin_r, sin_r, -sin_c, sin_c], 1), (1, 128 // HD))
+    hbm = pl.BlockSpec(memory_space=pl.ANY)
+    vmem = pl.BlockSpec(memory_space=pltpu.VMEM)
+    smem = pl.BlockSpec(memory_space=pltpu.SMEM)
+    dma = pltpu.SemaphoreType.DMA
+    bf16 = jnp.bfloat16
+    per_owner = nsp // ntp
+    return pl.pallas_call(
+        functools.partial(layer_kernel, nz, ntp),
+        out_shape=(
+            jax.ShapeDtypeStruct((rows, width), bf16),
+            jax.ShapeDtypeStruct((sink_logit.shape[0], rows), jnp.float32),
+        ),
+        in_specs=[hbm, vmem, hbm, hbm, hbm, hbm, vmem, smem, hbm, hbm, vmem, vmem],
+        out_specs=(vmem, vmem),
+        scratch_shapes=[
+            pltpu.VMEM((ntp, rows, width), bf16),
+            pltpu.VMEM((rows, dim), bf16),
+            pltpu.VMEM((dim, qn + 2 * kn + pn), bf16),
+            pltpu.VMEM((nsp, fan, ocols), bf16),
+            pltpu.VMEM((rows, qn), bf16),
+            pltpu.VMEM((rows + 2 * WINDOW, 2 * kn + pn), bf16),
+            pltpu.VMEM((rows, fan), bf16),
+            pltpu.VMEM((nsp, rows, ocols), bf16),
+            pltpu.VMEM((ntp, per_owner, rows, ocols), bf16),
+            dma((7,)),
+            dma((2, 3, nsp, PIECES)),
+            dma((2, nsp, PIECES)),
+            dma((ntp,)),
+            dma((ntp,)),
+            dma((2, 2)),
+            dma((2, 2)),
+            dma((nsp,)),
+            dma((ntp, per_owner)),
+        ],
+        compiler_params=pltpu.CompilerParams(
+            collective_id=0, has_side_effects=True, vmem_limit_bytes=56 << 20
+        ),
+    )(
+        tokens,
+        norm_gain[None, :],
+        query_weight,
+        key_weight,
+        value_weight,
+        pool_in_weight,
+        pool_mix_weight[0],
+        sink_logit,
+        out_pool_weight,
+        out_attn_weight,
+        cosine,
+        sine,
+    )
+
+
+def choose(mesh):
+    nsp, ntp = mesh.shape["sp"], mesh.shape["tp"]
+
+    def body(*args):
+        columns = args[8].shape[1]
+        fits = nsp % NY == 0 and nsp % ntp == 0 and columns % 128 == 0
+        if fits and args[0].shape[0] // WINDOW >= 2:
+            return fused(nsp // NY, ntp, *args)
+        return local(*args)
+
+    return body
+
+
 def solution(mesh):
     return jax.shard_map(
-        local,
+        choose(mesh),
         mesh=mesh,
         in_specs=(
             P("sp", "tp"),

time: 263 us -> 118 us (0.45)
  waiting for transfers between devices: 149 us -> 0 us
  Pallas kernels: 0 us -> 112 us
  blocking collectives: 48.5 us -> 0 us
  matrix products: 27.3 us -> 0 us
  between operations: 14.6 us -> 0.69 us
  starting transfers between devices: 12.8 us -> 0 us
  other arithmetic: 7.62 us -> 0.36 us
  local copies, waits for them, and re-layouts: 0.88 us -> 4.18 us
    all_gather x5 -> x0, waiting for transfers between devices: 116 us -> none  [the longest x1 42.1 us: local(): lax.all_gather(weights_in[0], 'sp', axis=0, tiled=True)]
    pallas_call x0 -> x1, Pallas kernels: none -> 112 us  [fused(): pl.pallas_call(functools.partial(layer_kernel, nz, ntp), out_shape=(jax.S...]
    all_gather x2 -> x0, blocking collectives: 48.5 us -> none  [the longest x1 26.4 us: local(): lax.all_gather(weights_in[2], 'sp', axis=0, tiled=True)]
    reduce_scatter x1 -> x0, waiting for transfers between devices: 29.3 us -> none  [local(): lax.psum_scatter(term.astype(jnp.bfloat16), 'tp', scatter_dimension=1, ti...]
    dot_general x10 -> x0, matrix products: 27.3 us -> none  [the longest x4 9.07 us: local(): jnp.dot(normed, piece, preferred_element_type=jnp.float32)]
    ppermute x4 -> x0, starting transfers between devices: 12.5 us -> none  [the longest x2 7.7 us: with_halo(): lax.ppermute(head, axis, [((i + 1) % count, i) for i in range(ends)])]
    reduce_sum x3 -> x0, other arithmetic: 4 us -> none  [the longest x1 2.23 us: local(): jnp.mean(wide * wide, -1, keepdims=True) + norm_eps]
    unnamed x6 -> x0, waiting for transfers between devices: 3.13 us -> none
  transfers between devices with their start and end apart: 10 -> 0, of which waited for: 5 -> 0; matrix products, arithmetic and copies ran while one was open for 12% -> 0% of each run, Pallas kernels for 0% -> 0%
where the time goes in v1:
time: 118 us; the launch traced here: 117 us
  Pallas kernels  112 us (95%)
  local copies, waits for them, and re-layouts  4.18 us (4%)
    pallas_call x1, Pallas kernels, fused(): pl.pallas_call(functools.partial(layer_kernel, nz, ntp), out_shape=(jax.S...  112 us
    unnamed x4, local copies, waits for them, and re-layouts  2.48 us

profile of v1, /device:TPU:19, one launch (start us, length us, event | category | flops | bytes accessed | tf_op | source)
XLA Modules:
  0.0 117.4 jit_solution(7915702011266142467)
XLA Ops:
  0.7 0.3 fusion
  1.0 0.8 copy.13.sin_ref
  1.9 0.8 copy.12.cos_ref
  2.7 112.2 %shard_map.113 = (bf16[512,512]{1,0:T(8,128)(2,1)}, f32[8,512]{1,0:T(8,128)}) custom-call(bf16[512,512]{1,0:T(8,128)(2,1)} %tok_ref.1, f32[1,2048]{1,0:T(1,128)} %bitcast.7, bf16[256,512]{1,0:T(8,128)(2,1)} %qw_ref.1, bf16[256,128]{1,0:T(8,128)(2,1)} %kw_ref.1, bf16[256,128]{1,0:T(8,128)(2,1)} %vw_ref.1, bf16[256,256]{1,0:T(8,128)(2,1)} %pw_ref.1, ...), custom_call_target="tpu_custom_call" | custom-call | tf_op jit(solution)/shard_map/pallas_call | solution.py:616
  114.9 0.0 copy-start
  114.9 1.9 %copy.16 = bf16[512,512]{1,0:T(8,128)(2,1)} copy(bf16[512,512]{1,0:T(8,128)(2,1)} %get-tuple-element.15) | data formatting | bytes 1048576
  116.8 0.0 copy-done
  116.8 0.6 copy.17
  (6 shorter events, 0.1 us)
Async XLA Ops:
  114.9 1.9 %copy-start = (f32[8,512]{1,0:T(8,128)S(1)}, f32[8,512]{1,0:T(8,128)}, u32[]{:S(2)}) copy-start(f32[8,512]{1,0:T(8,128)} %get-tuple-element.16) | copy-start | bytes 49156

commit v2 on v1

--- a/solution.py
+++ b/solution.py
@@ -1,4 +1,5 @@
 import functools
+import math
 
 import jax
 import jax.numpy as jnp
@@ -190,7 +191,7 @@
 
 
 NY = 2
-PIECES = 2
+PIECES = 4
 MESH = pl.DeviceIdType.MESH
 
 
@@ -207,8 +208,6 @@
     sink_ref,
     ow_ref,
     aw_ref,
-    cos_ref,
-    sin_ref,
     mixed_ref,
     log_ref,
     xg,
@@ -220,6 +219,10 @@
     act,
     part,
     rsb,
+    cos_ref,
+    sin_ref,
+    pair,
+    total_out,
     loc_sem,
     w_send,
     w_recv,
@@ -229,6 +232,8 @@
     h_recv,
     r_send,
     r_recv,
+    p_send,
+    p_recv,
 ):
     sp, tp = lax.axis_index("sp"), lax.axis_index("tp")
     nsp = nz * NY
@@ -302,37 +307,67 @@
 
     onward = (z + 1 < nz, z >= 1)
 
+    def issue(copy, done):
+        if done:
+            copy.wait_send()
+        else:
+            copy.start()
+
+    last = PIECES - 1
+
     def relay(kind, d, done=False):
-        def act_on(copy):
-            if done:
-                copy.wait_send()
-            else:
-                copy.start()
-
         for piece in range(PIECES):
             for way in range(2):
                 source = (z - d, z + d)[way]
                 block = source * NY + y
-                if d == 0:
+                valid = (source >= 0) & (source < nz)
+
+                @pl.when(valid)
+                def _():
+                    if not done:
+                        weight_copy(kind, block, piece, 2).wait_recv()
+
                     @pl.when(onward[way])
                     def _():
-                        act_on(weight_copy(kind, block, piece, way))
-
-                    if way == 1:
-                        act_on(weight_copy(kind, block, piece, 2))
-                else:
-                    valid = (source >= 0) & (source < nz)
-
-                    @pl.when(valid)
+                        issue(weight_copy(kind, block, piece, way), done)
+
+                    if kind == 1 or piece != last:
+                        issue(weight_copy(kind, block, piece, 2), done)
+
+    def own_row(kind, way, done=False):
+        for piece in range(PIECES):
+            if way == 2:
+                issue(weight_copy(kind, sp, piece, way), done)
+            else:
+
+                @pl.when(onward[way])
+                def _():
+                    issue(weight_copy(kind, sp, piece, way), done)
+
+    def relay_other(d, done=False):
+        if d == 0:
+            block = z * NY + (1 - y)
+            if not done:
+                weight_copy(0, block, last, 2).wait_recv()
+            for way in range(2):
+
+                @pl.when(onward[way])
+                def _():
+                    issue(weight_copy(0, block, last, way), done)
+
+        else:
+            for way in range(2):
+                source = (z - d, z + d)[way]
+
+                @pl.when((source >= 0) & (source < nz))
+                def _():
+                    block = source * NY + (1 - y)
+                    if not done:
+                        weight_copy(0, block, last, 2).wait_recv()
+
+                    @pl.when(onward[way])
                     def _():
-                        if not done:
-                            weight_copy(kind, block, piece, 2).wait_recv()
-
-                        @pl.when(onward[way])
-                        def _():
-                            act_on(weight_copy(kind, block, piece, way))
-
-                        act_on(weight_copy(kind, block, piece, 2))
+                        issue(weight_copy(0, block, last, way), done)
 
     def token_copy(step):
         other = lax.rem(tp + step, ntp)
@@ -356,11 +391,42 @@
             device_id_type=MESH,
         )
 
-    relay(0, 0)
+    for piece in range(PIECES):
+        for way in range(2):
+
+            @pl.when(onward[way])
+            def _():
+                weight_copy(0, sp, piece, way).start()
+
+        weight_copy(0, sp, piece, 2).start()
     for step in range(1, ntp):
         token_copy(step).start()
+
+    def out_starts(d):
+        @pl.when(z == d)
+        def _():
+            own_row(1, 0)
+
+        @pl.when(nz - 1 - z == d)
+        def _():
+            own_row(1, 1)
+
+    half = HD // 4
+    lane = lax.broadcasted_iota(jnp.int32, (rows, 128), 1)
+    is_first = (lane % (2 * half)) < half
+    position = sp * rows + lax.broadcasted_iota(jnp.int32, (rows, 128), 0)
+    place = jnp.where((lane % HD) < 2 * half, position // GRID_W, position % GRID_W)
+    freqs = jnp.exp((lane % half).astype(jnp.float32) * (-math.log(rope_base) / half))
+    angle = place.astype(jnp.float32) * freqs
+    cos_ref[...] = jnp.cos(angle)
+    sine = jnp.sin(angle)
+    sin_ref[...] = jnp.where(is_first, -sine, sine)
+
     for d in range(1, nz - 1):
         relay(0, d)
+        relay_other(d - 1)
+        out_starts(d - 1)
+    own_row(1, 2)
 
     for step in range(1, ntp):
         token_wait(step).wait_recv()
@@ -379,17 +445,13 @@
 
     for d in range(max(nz - 1, 1), nz):
         relay(0, d)
-    relay(1, 0)
-    for d in range(1, min(nz, 2)):
-        relay(1, d)
+    for d in range(max(nz - 2, 0), nz):
+        relay_other(d)
+        out_starts(d)
 
     for source in range(nz):
-        for piece in range(PIECES):
+        for piece in range(PIECES - 1):
             weight_copy(0, source * NY + (1 - y), piece, 2).wait_recv()
-
-    half = HD // 4
-    lane = lax.broadcasted_iota(jnp.int32, (rows, 128), 1)
-    is_first = (lane % (2 * half)) < half
 
     def turn(values, factor):
         wide = values.astype(jnp.bfloat16).astype(jnp.float32)
@@ -439,6 +501,9 @@
             halo_copy(way, 0).start()
             halo_copy(way, 1).start()
 
+    for d in range(1, min(nz, 2)):
+        relay(1, d)
+
     span = 3 * WINDOW
     row_at = lax.broadcasted_iota(jnp.int32, (WINDOW, span), 0)
     key_at = lax.broadcasted_iota(jnp.int32, (WINDOW, span), 1)
@@ -461,7 +526,7 @@
         own_pool = ext[(i + 1) * WINDOW : (i + 2) * WINDOW, 2 * kn : 2 * kn + pn]
         pooled = (summed / counted - own_pool.astype(jnp.float32)).astype(jnp.bfloat16)
         act[q_at, 0:pn] = jnp.dot(
-            pooled, mix_ref[...], preferred_element_type=jnp.float32
+            pooled, mix_ref[0], preferred_element_type=jnp.float32
         ).astype(jnp.bfloat16)
         valid = inside & (apart >= 0) & (apart <= 2 * WINDOW)
         logs = jnp.zeros((WINDOW, 128), jnp.float32)
@@ -494,9 +559,8 @@
     n_blocks = rows // WINDOW
     for i in range(1, n_blocks - 1):
         mixer_block(i)
-        if i == 1:
-            for d in range(2, min(nz, 3)):
-                relay(1, d)
+    for d in range(2, min(nz, 3)):
+        relay(1, d)
     for way, ok in ((0, has_prev), (1, has_next)):
         @pl.when(ok)
         def _():
@@ -505,21 +569,41 @@
 
     for i in (0, n_blocks - 1):
         mixer_block(i)
-        if i == 0:
-            for d in range(3, nz):
-                relay(1, d)
 
     per_owner = nsp // ntp
 
-    def reduce_copy(block):
-        owner = block // per_owner
+    mate = tp + 1 - 2 * (tp % 2)
+
+    def on_chip(block):
+        return (block // per_owner) // 2 == tp // 2
+
+    def is_mine(block):
+        return block // per_owner == tp
+
+    def is_joined(block):
+        return jnp.logical_not(on_chip(block)) & ((block // per_owner) % 2 == tp % 2)
+
+    def is_lent(block):
+        return jnp.logical_not(on_chip(block)) & ((block // per_owner) % 2 != tp % 2)
+
+    def reduce_copy(block, source):
         slot = block % per_owner
         return pltpu.make_async_remote_copy(
-            src_ref=part.at[block],
+            src_ref=source.at[block],
             dst_ref=rsb.at[tp, slot],
             send_sem=r_send.at[block],
             recv_sem=r_recv.at[tp, slot],
-            device_id={"tp": owner},
+            device_id={"tp": block // per_owner},
+            device_id_type=MESH,
+        )
+
+    def lend_copy(block):
+        return pltpu.make_async_remote_copy(
+            src_ref=part.at[block],
+            dst_ref=pair.at[block],
+            send_sem=p_send.at[block],
+            recv_sem=p_recv.at[block],
+            device_id={"tp": mate},
             device_id_type=MESH,
         )
 
@@ -528,29 +612,60 @@
             jnp.bfloat16
         )
 
-        @pl.when(block // per_owner != tp)
-        def _():
-            reduce_copy(block).start()
-
-    @pl.loop(0, nz)
-    def _(j):
-        out_block(j * NY + y)
-
-    @pl.loop(0, 2 * nz - 1)
-    def _(k):
-        d = (k + 1) // 2
-        source = z + (1 - 2 * (k % 2)) * d
-
-        @pl.when((source >= 0) & (source < nz))
-        def _():
-            block = source * NY + (1 - y)
-            for piece in range(PIECES):
-                weight_copy(1, block, piece, 2).wait_recv()
-            out_block(block)
-
-    for step in range(1, ntp):
-        other = lax.rem(tp + step, ntp)
-        for slot in range(per_owner):
+        @pl.when(on_chip(block) & jnp.logical_not(is_mine(block)))
+        def _():
+            reduce_copy(block, part).start()
+
+        @pl.when(is_lent(block))
+        def _():
+            lend_copy(block).start()
+
+    def join_block(block):
+        @pl.when(is_joined(block))
+        def _():
+            lend_copy(block).wait_recv()
+            total_out[block] = (
+                part[block].astype(jnp.float32) + pair[block].astype(jnp.float32)
+            ).astype(jnp.bfloat16)
+            reduce_copy(block, total_out).start()
+
+    def row_steps(low, high):
+        @pl.loop(2 * low, 2 * high)
+        def _(k):
+            d = k // 2
+            source = z + (2 * (k % 2) - 1) * d
+
+            @pl.when((source >= 0) & (source < nz) & ((d > 0) | (k % 2 == 0)))
+            def _():
+                out_block(source * NY + y)
+                join_block(source * NY + y)
+
+    def other_steps(low, high):
+        @pl.loop(2 * low, 2 * high)
+        def _(k):
+            d = k // 2
+            source = z + (2 * (k % 2) - 1) * d
+
+            @pl.when((source >= 0) & (source < nz) & ((d > 0) | (k % 2 == 0)))
+            def _():
+                block = source * NY + (1 - y)
+                for piece in range(PIECES):
+                    weight_copy(1, block, piece, 2).wait_recv()
+                out_block(block)
+                join_block(block)
+
+    near = min(nz, 3)
+    row_steps(0, near)
+    other_steps(0, min(nz, 2))
+    for d in range(3, nz):
+        relay(1, d)
+    row_steps(near, nz)
+    other_steps(min(nz, 2), nz)
+
+    for slot in range(per_owner):
+        total = part[tp * per_owner + slot].astype(jnp.float32)
+        for step in range(ntp // 2):
+            other = mate if step == 0 else lax.rem(tp + 2 * step, ntp)
             pltpu.make_async_remote_copy(
                 src_ref=rsb.at[other, slot],
                 dst_ref=rsb.at[other, slot],
@@ -559,17 +674,18 @@
                 device_id={"tp": other},
                 device_id_type=MESH,
             ).wait_recv()
-    for slot in range(per_owner):
-        total = part[tp * per_owner + slot].astype(jnp.float32)
-        for step in range(1, ntp):
-            total = total + rsb[lax.rem(tp + step, ntp), slot].astype(jnp.float32)
+            total = total + rsb[other, slot].astype(jnp.float32)
         mixed_ref[:, slot * ocols : (slot + 1) * ocols] = total.astype(jnp.bfloat16)
 
     for step in range(1, ntp):
         token_copy(step).wait_send()
     for kind in range(2):
-        for d in range(nz):
+        for way in range(3):
+            own_row(kind, way, done=True)
+        for d in range(1, nz):
             relay(kind, d, done=True)
+    for d in range(nz):
+        relay_other(d, done=True)
     for way, ok in ((0, has_next), (1, has_prev)):
         @pl.when(ok)
         def _():
@@ -578,9 +694,13 @@
 
     @pl.loop(0, nsp)
     def _(block):
-        @pl.when(block // per_owner != tp)
-        def _():
-            reduce_copy(block).wait_send()
+        @pl.when((on_chip(block) & jnp.logical_not(is_mine(block))) | is_joined(block))
+        def _():
+            reduce_copy(block, part).wait_send()
+
+        @pl.when(is_lent(block))
+        def _():
+            lend_copy(block).wait_send()
 
 
 def fused(
@@ -603,10 +723,6 @@
     qn, kn, pn = query_weight.shape[1], key_weight.shape[1], pool_in_weight.shape[1]
     fan = out_pool_weight.shape[0] + out_attn_weight.shape[0]
     ocols = out_pool_weight.shape[1]
-    positions = lax.axis_index("sp") * rows + jnp.arange(rows, dtype=jnp.int32)
-    cos_r, sin_r, cos_c, sin_c = rope_tables(positions, HD)
-    cosine = jnp.tile(jnp.concatenate([cos_r, cos_r, cos_c, cos_c], 1), (1, 128 // HD))
-    sine = jnp.tile(jnp.concatenate([-sin_r, sin_r, -sin_c, sin_c], 1), (1, 128 // HD))
     hbm = pl.BlockSpec(memory_space=pl.ANY)
     vmem = pl.BlockSpec(memory_space=pltpu.VMEM)
     smem = pl.BlockSpec(memory_space=pltpu.SMEM)
@@ -619,7 +735,7 @@
             jax.ShapeDtypeStruct((rows, width), bf16),
             jax.ShapeDtypeStruct((sink_logit.shape[0], rows), jnp.float32),
         ),
-        in_specs=[hbm, vmem, hbm, hbm, hbm, hbm, vmem, smem, hbm, hbm, vmem, vmem],
+        in_specs=[hbm, vmem, hbm, hbm, hbm, hbm, vmem, smem, hbm, hbm],
         out_specs=(vmem, vmem),
         scratch_shapes=[
             pltpu.VMEM((ntp, rows, width), bf16),
@@ -631,6 +747,10 @@
             pltpu.VMEM((rows, fan), bf16),
             pltpu.VMEM((nsp, rows, ocols), bf16),
             pltpu.VMEM((ntp, per_owner, rows, ocols), bf16),
+            pltpu.VMEM((rows, 128), jnp.float32),
+            pltpu.VMEM((rows, 128), jnp.float32),
+            pltpu.VMEM((nsp, rows, ocols), bf16),
+            pltpu.VMEM((nsp, rows, ocols), bf16),
             dma((7,)),
             dma((2, 3, nsp, PIECES)),
             dma((2, nsp, PIECES)),
@@ -640,6 +760,8 @@
             dma((2, 2)),
             dma((nsp,)),
             dma((ntp, per_owner)),
+            dma((nsp,)),
+            dma((nsp,)),
         ],
         compiler_params=pltpu.CompilerParams(
             collective_id=0, has_side_effects=True, vmem_limit_bytes=56 << 20
@@ -651,12 +773,10 @@
         key_weight,
         value_weight,
         pool_in_weight,
-        pool_mix_weight[0],
+        pool_mix_weight,
         sink_logit,
         out_pool_weight,
         out_attn_weight,
-        cosine,
-        sine,
     )
 
 
@@ -665,7 +785,7 @@
 
     def body(*args):
         columns = args[8].shape[1]
-        fits = nsp % NY == 0 and nsp % ntp == 0 and columns % 128 == 0
+        fits = nsp % NY == 0 and nsp % ntp == 0 and columns % 128 == 0 and ntp % 2 == 0
         if fits and args[0].shape[0] // WINDOW >= 2:
             return fused(nsp // NY, ntp, *args)
         return local(*args)

time: 118 us -> 99.3 us (0.84)
  the two profiles are of different devices: /device:TPU:19 before, /device:TPU:24 now
where the time goes in v2:
time: 99.3 us; the launch traced here: 99.1 us
  Pallas kernels  96 us (97%)
  local copies, waits for them, and re-layouts  2.48 us (2%)
    pallas_call x1, Pallas kernels, fused(): pl.pallas_call(functools.partial(layer_kernel, nz, ntp), out_shape=(jax.S...  96 us
    unnamed x4, local copies, waits for them, and re-layouts  2.48 us

profile of v2, /device:TPU:24, one launch (start us, length us, event | category | flops | bytes accessed | tf_op | source)
XLA Modules:
  0.0 99.1 jit_solution(4426766326669799865)
XLA Ops:
  0.6 96.0 %shard_map.113 = (bf16[512,512]{1,0:T(8,128)(2,1)}, f32[8,512]{1,0:T(8,128)}) custom-call(bf16[512,512]{1,0:T(8,128)(2,1)} %tok_ref.1, f32[1,2048]{1,0:T(1,128)} %bitcast.1, bf16[256,512]{1,0:T(8,128)(2,1)} %qw_ref.1, bf16[256,128]{1,0:T(8,128)(2,1)} %kw_ref.1, bf16[256,128]{1,0:T(8,128)(2,1)} %vw_ref.1, bf16[256,256]{1,0:T(8,128)(2,1)} %pw_ref.1, ...), custom_call_target="tpu_custom_call" | custom-call | tf_op jit(solution)/shard_map/pallas_call | solution.py:732
  96.6 0.0 copy-start
  96.6 1.9 %copy.14 = bf16[512,512]{1,0:T(8,128)(2,1)} copy(bf16[512,512]{1,0:T(8,128)(2,1)} %get-tuple-element.4) | data formatting | bytes 1048576
  98.5 0.0 copy-done
  98.5 0.6 copy.15
Async XLA Ops:
  96.6 1.9 %copy-start = (f32[8,512]{1,0:T(8,128)S(1)}, f32[8,512]{1,0:T(8,128)}, u32[]{:S(2)}) copy-start(f32[8,512]{1,0:T(8,128)} %get-tuple-element.5) | copy-start | bytes 49156
